TPU v7x, 256 devices: a whole 4x4x8 slice. The times are simulated.
256 devices in a mesh: ep: 32 (over z, x), tp: 8 (over y, core).
Axes of the slice: x: 4, y: 4, z: 8, core: 2. Of those that a mesh axis runs over, the one named last changes fastest.
Arguments:
- tokens: bfloat16 [32768, 2048], P(('ep', 'tp')), may hold values from -24 to 24
- expert_ids: int32 [32768, 4], P(('ep', 'tp')), may hold values from 0 to 31, all different within a row; in each aligned block of 128 rows (0 to 127, 128 to 255, ...) at most 24 rows name the same one
- route_weights: float32 [32768, 4], P(('ep', 'tp')), may hold values from 0.2 to 1.2
- cotangent: bfloat16 [32768, 2048], P(('ep', 'tp')), may hold values from -24 to 24
- gate_weight: bfloat16 [256, 512, 2048], P(('ep', 'tp')), may hold values from -0.125 to 0.125
- up_weight: bfloat16 [256, 512, 2048], P(('ep', 'tp')), may hold values from -0.125 to 0.125
- down_weight: bfloat16 [256, 512, 2048], P(('ep', 'tp')), may hold values from -0.25 to 0.25
- shared_gate: bfloat16 [256, 2048], replicated, may hold values from -0.125 to 0.125
- shared_up: bfloat16 [256, 2048], replicated, may hold values from -0.125 to 0.125
- shared_down: bfloat16 [256, 2048], replicated, may hold values from -0.375 to 0.375
Outputs:
- token_grad: bfloat16 [32768, 2048], P(('ep', 'tp'))
- route_grad: float32 [32768, 4], P(('ep', 'tp'))
- gate_grad: bfloat16 [256, 512, 2048], P(('ep', 'tp'))
- up_grad: bfloat16 [256, 512, 2048], P(('ep', 'tp'))
- down_grad: bfloat16 [256, 512, 2048], P(('ep', 'tp'))
- shared_grads: float32 [2048, 3, 256], P(('ep', 'tp'))
Inputs may be any that keep to these rules, and one draw needn't show every extreme that they name: `expert_ids`: each row names 4 different numbers of 0 to 31, experts within the group of the row's device. Among the rows of one device (aligned blocks of 128 tokens) no number is named more than 24 times, and in some blocks one number is named exactly 24 times.
All inputs are finite; a program needn't handle non-finite values.
Results may differ from a plain program's by a relative error of at most 0.006.
Values may be sent and summed in bfloat16 or wider, within the bound.
A program may use at most 128 MiB of HBM per device.

v0:
```python
import jax
import jax.numpy as jnp
from jax import lax
from jax.sharding import PartitionSpec as P


def gated_backward(scaled, gate_pre, up_pre):
    sigmoid_gate = jax.nn.sigmoid(gate_pre)
    gate_delta = (scaled * up_pre * sigmoid_gate * (1.0 + gate_pre * (1.0 - sigmoid_gate))).astype(
        jnp.bfloat16
    )
    up_delta = (scaled * jax.nn.silu(gate_pre)).astype(jnp.bfloat16)
    return (gate_delta, up_delta)


def forward_products(token_rows, gate_local, up_local):
    gate_pre = jnp.einsum("rd,fd->rf", token_rows, gate_local, preferred_element_type=jnp.float32)
    up_pre = jnp.einsum("rd,fd->rf", token_rows, up_local, preferred_element_type=jnp.float32)
    return (gate_pre, up_pre)


def shards(
    tokens,
    expert_ids,
    route_weights,
    cotangent,
    gate_weight,
    up_weight,
    down_weight,
    shared_gate,
    shared_up,
    shared_down,
):
    ep_size = lax.axis_size("ep")
    tok_rows = tokens.shape[0]
    model_width = tokens.shape[1]
    top_count = expert_ids.shape[1]
    capacity = 3 * tok_rows * top_count // (2 * ep_size)
    slots_all = ep_size * capacity
    assign_count = tok_rows * top_count
    flat_ids = expert_ids.reshape(-1)
    one_hot = (flat_ids[:, None] == jnp.arange(ep_size, dtype=jnp.int32)[None, :]).astype(jnp.int32)
    slot_index = jnp.sum(jnp.cumsum(one_hot, axis=0) * one_hot, axis=1) - 1
    position = flat_ids * capacity + slot_index
    row_assign = (
        jnp.full((slots_all,), assign_count, jnp.int32)
        .at[position]
        .set(jnp.arange(assign_count, dtype=jnp.int32))
    )
    row_token = row_assign // top_count
    row_weight = jnp.take(
        jnp.concatenate([route_weights.reshape(-1), jnp.zeros((1,), jnp.float32)], axis=0),
        row_assign,
        axis=0,
    )
    empty_row = jnp.zeros((1, model_width), jnp.bfloat16)
    send_tokens = jnp.take(jnp.concatenate([tokens, empty_row], axis=0), row_token, axis=0).reshape(
        ep_size, capacity, model_width
    )
    send_cot = jnp.take(jnp.concatenate([cotangent, empty_row], axis=0), row_token, axis=0).reshape(
        ep_size, capacity, model_width
    )
    gate_local = gate_weight[0]
    up_local = up_weight[0]
    down_local = down_weight[0]
    scales = lax.all_to_all(
        row_weight.reshape(ep_size, capacity), "ep", split_axis=0, concat_axis=0, tiled=True
    ).reshape(slots_all)
    token_rows, cot_rows = (
        lax.all_to_all(send_tokens, "ep", split_axis=0, concat_axis=0, tiled=True),
        lax.all_to_all(send_cot, "ep", split_axis=0, concat_axis=0, tiled=True),
    )
    token_rows = token_rows.reshape(slots_all, model_width)
    cot_rows = cot_rows.reshape(slots_all, model_width)
    gate_pre, up_pre = forward_products(token_rows, gate_local, up_local)
    hidden = (jax.nn.silu(gate_pre) * up_pre).astype(jnp.bfloat16)
    back_hidden = jnp.einsum("rd,fd->rf", cot_rows, down_local, preferred_element_type=jnp.float32)
    route_part = jnp.sum(back_hidden * hidden.astype(jnp.float32), axis=1)
    gate_delta, up_delta = gated_backward(scales[:, None] * back_hidden, gate_pre, up_pre)
    weighted_cot = (scales[:, None] * cot_rows.astype(jnp.float32)).astype(jnp.bfloat16)
    token_part = jnp.einsum(
        "rf,fd->rd", gate_delta, gate_local, preferred_element_type=jnp.float32
    ) + jnp.einsum("rf,fd->rd", up_delta, up_local, preferred_element_type=jnp.float32)
    gate_grad = jnp.einsum(
        "rf,rd->fd", gate_delta, token_rows, preferred_element_type=jnp.float32
    ).astype(jnp.bfloat16)[None]
    up_grad = jnp.einsum(
        "rf,rd->fd", up_delta, token_rows, preferred_element_type=jnp.float32
    ).astype(jnp.bfloat16)[None]
    down_grad = jnp.einsum(
        "rf,rd->fd", hidden, weighted_cot, preferred_element_type=jnp.float32
    ).astype(jnp.bfloat16)[None]
    back_rows, back_route = (
        lax.all_to_all(
            token_part.reshape(ep_size, capacity, model_width),
            "ep",
            split_axis=0,
            concat_axis=0,
            tiled=True,
        ),
        lax.all_to_all(
            route_part.reshape(ep_size, capacity), "ep", split_axis=0, concat_axis=0, tiled=True
        ),
    )
    routed = jnp.sum(
        jnp.take(back_rows.reshape(slots_all, model_width), position, axis=0).reshape(
            tok_rows, top_count, model_width
        ),
        axis=1,
    )
    route_grad = jnp.take(back_route.reshape(slots_all), position, axis=0).reshape(
        tok_rows, top_count
    )
    common_gate = jnp.einsum("td,fd->tf", tokens, shared_gate, preferred_element_type=jnp.float32)
    common_up = jnp.einsum("td,fd->tf", tokens, shared_up, preferred_element_type=jnp.float32)
    common_hidden = (jax.nn.silu(common_gate) * common_up).astype(jnp.bfloat16)
    common_back = jnp.einsum(
        "td,fd->tf", cotangent, shared_down, preferred_element_type=jnp.float32
    )
    common_gate_delta, common_up_delta = gated_backward(common_back, common_gate, common_up)
    common_part = jnp.einsum(
        "tf,fd->td", common_gate_delta, shared_gate, preferred_element_type=jnp.float32
    ) + jnp.einsum("tf,fd->td", common_up_delta, shared_up, preferred_element_type=jnp.float32)
    shared_grads = lax.psum_scatter(
        jnp.stack(
            [
                jnp.einsum(
                    "tc,tf->cf", tokens, common_gate_delta, preferred_element_type=jnp.float32
                ),
                jnp.einsum(
                    "tc,tf->cf", tokens, common_up_delta, preferred_element_type=jnp.float32
                ),
                jnp.einsum(
                    "tc,tf->cf", cotangent, common_hidden, preferred_element_type=jnp.float32
                ),
            ],
            axis=1,
        ),
        ("ep", "tp"),
        scatter_dimension=0,
        tiled=True,
    )
    token_grad = (routed + common_part).astype(jnp.bfloat16)
    return (token_grad, route_grad, gate_grad, up_grad, down_grad, shared_grads)


def solution(mesh):
    in_specs = (
        P(("ep", "tp"), None),
        P(("ep", "tp"), None),
        P(("ep", "tp"), None),
        P(("ep", "tp"), None),
        P(("ep", "tp"), None, None),
        P(("ep", "tp"), None, None),
        P(("ep", "tp"), None, None),
        P(),
        P(),
        P(),
    )
    out_specs = (
        P(("ep", "tp"), None),
        P(("ep", "tp"), None),
        P(("ep", "tp"), None, None),
        P(("ep", "tp"), None, None),
        P(("ep", "tp"), None, None),
        P(("ep", "tp"), None, None),
    )
    return jax.shard_map(shards, mesh=mesh, in_specs=in_specs, out_specs=out_specs, check_vma=False)
```

profile of v0, /device:TPU:6, one launch (start us, length us, event | category | flops | bytes accessed | tf_op | source)
XLA Modules:
  0.0 652.2 jit_solution(13074902463301345955)
XLA Ops:
  7.2 0.0 copy-start
  7.2 0.9 copy.25
  8.1 0.1 eq.26
  8.2 0.1 reshape.149
  8.4 1.2 reduce-window.6
  9.6 0.2 slice_reduce_fusion
  9.8 0.1 fusion.20
  9.9 0.1 mul.93
  10.1 2.4 scatter_custom_fusion
  12.6 0.8 copy.29
  13.3 0.1 reshape.151
  13.5 3.2 gather_fusion
  16.7 0.7 select_n.65
  17.4 11.6 %all-to-all-start = ((f32[32,1,24]{2,1,0:T(1,128)}), f32[32,1,24]{2,1,0:T(1,128)S(1)}, u32[]{:S(2)}, u32[]{:S(2)}) async-start(f32[32,1,24]{2,1,0:T(1,128)} %bitcast.3), calls=%async_computation | async-start | bytes 32768 | tf_op jit(solution)/shard_map/all_to_all | solution.py:66
  29.0 1.1 concatenate.11
  30.1 4.3 gather_fusion.4
  34.4 4.3 gather_fusion.3
  38.7 5.0 broadcast_select_fusion.1
  43.6 82.3 %all_to_all.30 = bf16[32,24,2048]{2,1,0:T(8,128)(2,1)} all-to-all(bf16[32,24,2048]{2,1,0:T(8,128)(2,1)} %bitcast.86), channel_id=1, replica_groups=mesh['ep'=32,'tp'=8] {'ep'}, dimensions={0} | all-to-all | bytes 6291456 | tf_op jit(solution)/shard_map/all_to_all | solution.py:70
  126.0 5.6 all-to-all-start.1
  131.6 0.5 broadcast.165
  132.1 0.7 reduce.8
  132.8 0.1 mul.94
  132.9 5.0 fusion.10
  137.9 3.0 fusion.13
  140.9 62.5 %all-to-all-done.1 = bf16[32,24,2048]{2,1,0:T(8,128)(2,1)} async-done(((bf16[32,24,2048]{2,1,0:T(8,128)(2,1)}), bf16[32,24,2048]{2,1,0:T(8,128)(2,1)}, u32[]{:S(2)}, u32[]{:S(2)}) %all-to-all-start.1) | async-done | bytes 3145760 | tf_op jit(solution)/shard_map/all_to_all | solution.py:71
  203.4 7.0 %multiply_reduce_fusion = (f32[768]{0:T(1024)S(1)}, bf16[768,512]{0,1:T(8,128)(2,1)}, bf16[768,512]{0,1:T(8,128)(2,1)}, bf16[768,512]{0,1:T(8,128)(2,1)S(1)}) fusion(f32[768,512]{0,1:T(8,128)} %fusion.13, f32[768,512]{0,1:T(8,128)} %fusion.10, f32[768]{0:T(1024)S(1)} %mul.94, bf16[768,2048]{1,0:T(8,128)(2,1)} %bitcast.5, bf16[1,512,2048]{2,1,0:T(8,128)(2,1)} %param.18), kind=kOutput, calls=%fused_computation.35 | convolution fusion | flops 1618083072 | bytes 10754048 | tf_op jit(solution)/shard_map/rd,fd->rf/dot_general | solution.py:77
  210.4 0.8 all_to_all.23
  211.2 5.6 all-to-all-start.4
  216.8 0.0 copy-start.10
  216.8 3.1 fusion.8
  220.0 4.5 convolution_add_fusion
  224.4 0.3 all-to-all-done.4
  224.7 9.7 %all-to-all-start.3 = ((f32[32,24,2048]{2,1,0:T(8,128)}), f32[32,24,2048]{2,1,0:T(8,128)}, u32[]{:S(2)}, u32[]{:S(2)}) async-start(f32[32,24,2048]{2,1,0:T(8,128)} %bitcast.84), calls=%async_computation.3 | async-start | bytes 12582912 | tf_op jit(solution)/shard_map/all_to_all | solution.py:94
  234.4 0.0 all-reduce.5.cloned.1.call-start
  234.5 0.5 fusion.29
  235.0 0.5 fusion.28
  235.5 0.3 copy-done.17
  235.8 0.5 multiply_convert_fusion.10
  236.3 0.5 convolution_bitcast_fusion.2
  236.8 0.5 convolution_bitcast_fusion.1
  237.3 0.1 copy-done.13
  237.4 0.5 convolution_bitcast_fusion
  237.9 3.3 pad_maximum_fusion
  241.1 9.1 %copy.32 = f32[2048,3,256]{2,1,0:T(4,128)} copy(f32[2048,3,256]{0,2,1:T(8,128)} %pad_maximum_fusion) | data formatting | bytes 12582912 | tf_op jit(solution)/shard_map/stack | solution.py:125
  250.2 0.0 all-reduce.5.cloned.1.call-update
  250.3 0.1 sub.21
  250.4 1.1 copy-done.6
  251.4 0.3 fusion.30
  251.8 354.7 %all-reduce.5.cloned.1.call-done = f32[2048,3,256]{2,1,0:T(4,128)} async-done(((f32[2048,3,256]{2,1,0:T(4,128)}), f32[2048,3,256]{2,1,0:T(4,128)}) %all-reduce.5.cloned.1.call-update) | async-done | bytes 6291472
  606.4 0.8 constant_dynamic-slice_fusion
  607.2 0.6 copy.34
  607.8 5.2 fusion.3
  613.0 3.2 fusion.4
  616.1 5.1 fusion.5
  621.3 0.7 reduce.9
  621.9 0.1 reshape.158
  622.0 2.3 gather_fusion.2
  624.3 0.1 gather.23
  624.5 0.7 copy.33
  625.1 8.2 %gather_fusion.1 = f32[512,2048]{1,0:T(8,128)} fusion(f32[768,2048]{1,0:T(8,128)} %bitcast.12, s32[1024]{0:T(1024)S(1)} %pad_clamp_fusion), kind=kCustom, calls=%fused_computation.3 | custom fusion | bytes 8390656 | tf_op jit(solution)/shard_map/jit(_take)/gather | solution.py:106
  633.3 5.2 gather.21
  638.5 5.7 select_reduce_fusion
  644.2 1.1 fusion.7
  (51 shorter events, 0.3 us)
Async XLA Ops:
  7.2 125.7 %copy-start = (bf16[1,512,2048]{2,1,0:T(8,128)(2,1)S(1)}, bf16[1,512,2048]{2,1,0:T(8,128)(2,1)}, u32[]{:S(2)}) copy-start(bf16[1,512,2048]{2,1,0:T(8,128)(2,1)} %param.16) | copy-start | bytes 6291460
  7.2 21.8 %copy-start.11 = (bf16[128,2048]{1,0:T(8,128)(2,1)S(1)}, bf16[128,2048]{1,0:T(8,128)(2,1)}, u32[]{:S(2)}) copy-start(bf16[128,2048]{1,0:T(8,128)(2,1)} %param.15) | copy-start | bytes 1572868
  17.4 26.3 %all-to-all-start = ((f32[32,1,24]{2,1,0:T(1,128)}), f32[32,1,24]{2,1,0:T(1,128)S(1)}, u32[]{:S(2)}, u32[]{:S(2)}) async-start(f32[32,1,24]{2,1,0:T(1,128)} %bitcast.3), calls=%async_computation | async-start | bytes 32768 | tf_op jit(solution)/shard_map/all_to_all | solution.py:66
  126.0 77.4 %all-to-all-start.1 = ((bf16[32,24,2048]{2,1,0:T(8,128)(2,1)}), bf16[32,24,2048]{2,1,0:T(8,128)(2,1)}, u32[]{:S(2)}, u32[]{:S(2)}) async-start(bf16[32,24,2048]{2,1,0:T(8,128)(2,1)} %bitcast.85), calls=%async_computation.1 | async-start | bytes 6291456 | tf_op jit(solution)/shard_map/all_to_all | solution.py:71
  132.9 5.0 copy-start.7
  132.9 5.0 copy-start.9
  210.4 9.5 %copy-start.14 = (bf16[768,512]{0,1:T(8,128)(2,1)}, bf16[768,512]{0,1:T(8,128)(2,1)S(1)}, u32[]{:S(2)}) copy-start(bf16[768,512]{0,1:T(8,128)(2,1)S(1)} %get-tuple-element.32) | copy-start | bytes 2359300
  211.2 13.5 %all-to-all-start.4 = ((f32[32,1,24]{2,1,0:T(1,128)}), f32[32,1,24]{2,1,0:T(1,128)S(1)}, u32[]{:S(2)}, u32[]{:S(2)}) async-start(f32[32,1,24]{2,1,0:T(1,128)} %bitcast.13), calls=%async_computation.4 | async-start | bytes 32768 | tf_op jit(solution)/shard_map/all_to_all | solution.py:101
  216.8 3.1 copy-start.10
  224.7 9.8 %copy-start.2 = (bf16[128,2048]{1,0:T(8,128)(2,1)S(1)}, bf16[128,2048]{1,0:T(8,128)(2,1)}, u32[]{:S(2)}) copy-start(bf16[128,2048]{1,0:T(8,128)(2,1)} %param.12) | copy-start | bytes 1572868
  224.7 9.8 %copy-start.5 = (bf16[256,2048]{1,0:T(8,128)(2,1)S(1)}, bf16[256,2048]{1,0:T(8,128)(2,1)}, u32[]{:S(2)}) copy-start(bf16[256,2048]{1,0:T(8,128)(2,1)} %param.19) | copy-start | bytes 3145732
  224.7 10.3 %copy-start.3 = (bf16[256,2048]{1,0:T(8,128)(2,1)S(1)}, bf16[256,2048]{1,0:T(8,128)(2,1)}, u32[]{:S(2)}) copy-start(bf16[256,2048]{1,0:T(8,128)(2,1)} %param.20) | copy-start | bytes 3145732
  224.7 400.4 %all-to-all-start.3 = ((f32[32,24,2048]{2,1,0:T(8,128)}), f32[32,24,2048]{2,1,0:T(8,128)}, u32[]{:S(2)}, u32[]{:S(2)}) async-start(f32[32,24,2048]{2,1,0:T(8,128)} %bitcast.84), calls=%async_computation.3 | async-start | bytes 12582912 | tf_op jit(solution)/shard_map/all_to_all | solution.py:94
  234.4 1.1 copy-start.12
  234.4 372.0 %all-reduce.5.cloned.1.call-start = ((), (), s32[]{:S(2)}) async-start(), calls=%async_computation.5 | async-start | bytes 16777216
  234.5 1.3 copy-start.17
  236.3 1.0 copy-start.13
  250.2 1.2 copy-start.6
  250.2 357.6 %copy-start.16 = (bf16[768,512]{0,1:T(8,128)(2,1)S(1)}, bf16[768,512]{0,1:T(8,128)(2,1)}, u32[]{:S(2)}) copy-start(bf16[768,512]{0,1:T(8,128)(2,1)} %get-tuple-element.31) | copy-start | bytes 2359300
  607.8 5.2 copy-start.8
  607.8 5.2 copy-start.15
  613.0 3.2 copy-start.18
  638.5 5.7 copy-start.4
  638.5 6.9 %copy-start.1 = (bf16[1,512,2048]{2,1,0:T(8,128)(2,1)S(1)}, bf16[1,512,2048]{2,1,0:T(8,128)(2,1)}, u32[]{:S(2)}) copy-start(bf16[1,512,2048]{2,1,0:T(8,128)(2,1)} %param.16) | copy-start | bytes 6291460
Sparse Core Ops, SparseCore 0:
  250.4 356.0 all-reduce.4
where the time goes:
time: 653 us; the launch traced here: 652 us
  waiting for transfers between devices  417 us (64%)
  blocking collectives  82.3 us (13%)
  local copies, waits for them, and re-layouts  48.5 us (7%)
  matrix products  40.3 us (6%)
  starting transfers between devices  32.5 us (5%)
  other arithmetic  16.7 us (3%)
  between operations  14.5 us (2%)
    unnamed x2, waiting for transfers between devices  355 us
    all_to_all x1, blocking collectives, shards(): lax.all_to_all(send_tokens, 'ep', split_axis=0, concat_axis=0, tiled=True)  82.3 us
    all_to_all x1, waiting for transfers between devices, shards(): lax.all_to_all(send_cot, 'ep', split_axis=0, concat_axis=0, tiled=True)  62.5 us
    gather x2, local copies, waits for them, and re-layouts, shards(): jnp.take(back_rows.reshape(slots_all, model_width), position, axis=0)  13.4 us
  transfers between devices with their start and end apart: 5, of which 3 were waited for; matrix products, arithmetic and copies ran while one was open for 10% of the time, Pallas kernels for 0%

commit v1 on v0

--- a/solution.py
+++ b/solution.py
@@ -92,7 +92,7 @@
     ).astype(jnp.bfloat16)[None]
     back_rows, back_route = (
         lax.all_to_all(
-            token_part.reshape(ep_size, capacity, model_width),
+            token_part.astype(jnp.bfloat16).reshape(ep_size, capacity, model_width),
             "ep",
             split_axis=0,
             concat_axis=0,
@@ -103,9 +103,9 @@
         ),
     )
     routed = jnp.sum(
-        jnp.take(back_rows.reshape(slots_all, model_width), position, axis=0).reshape(
-            tok_rows, top_count, model_width
-        ),
+        jnp.take(back_rows.reshape(slots_all, model_width), position, axis=0)
+        .reshape(tok_rows, top_count, model_width)
+        .astype(jnp.float32),
         axis=1,
     )
     route_grad = jnp.take(back_route.reshape(slots_all), position, axis=0).reshape(
@@ -121,25 +121,20 @@
     common_part = jnp.einsum(
         "tf,fd->td", common_gate_delta, shared_gate, preferred_element_type=jnp.float32
     ) + jnp.einsum("tf,fd->td", common_up_delta, shared_up, preferred_element_type=jnp.float32)
-    shared_grads = lax.psum_scatter(
-        jnp.stack(
-            [
-                jnp.einsum(
-                    "tc,tf->cf", tokens, common_gate_delta, preferred_element_type=jnp.float32
-                ),
-                jnp.einsum(
-                    "tc,tf->cf", tokens, common_up_delta, preferred_element_type=jnp.float32
-                ),
-                jnp.einsum(
-                    "tc,tf->cf", cotangent, common_hidden, preferred_element_type=jnp.float32
-                ),
-            ],
-            axis=1,
-        ),
-        ("ep", "tp"),
-        scatter_dimension=0,
-        tiled=True,
-    )
+    partial = jnp.stack(
+        [
+            jnp.einsum("tc,tf->cf", tokens, common_gate_delta, preferred_element_type=jnp.float32),
+            jnp.einsum("tc,tf->cf", tokens, common_up_delta, preferred_element_type=jnp.float32),
+            jnp.einsum("tc,tf->cf", cotangent, common_hidden, preferred_element_type=jnp.float32),
+        ],
+        axis=1,
+    ).astype(jnp.bfloat16)
+    tp_size = lax.axis_size("tp")
+    partial = partial.reshape(ep_size, tp_size, -1, 768).transpose(1, 0, 2, 3)
+    partial = lax.all_to_all(partial, "tp", split_axis=0, concat_axis=0, tiled=True)
+    partial = jnp.sum(partial.astype(jnp.float32), axis=0)
+    partial = lax.all_to_all(partial, "ep", split_axis=0, concat_axis=0, tiled=True)
+    shared_grads = jnp.sum(partial, axis=0).reshape(-1, 3, 256)
     token_grad = (routed + common_part).astype(jnp.bfloat16)
     return (token_grad, route_grad, gate_grad, up_grad, down_grad, shared_grads)
 

time: 653 us -> 392 us (0.60)
  waiting for transfers between devices: 417 us -> 140 us
  between operations: 14.5 us -> 1.04 us
  starting transfers between devices: 32.5 us -> 42.6 us
  matrix products: 40.3 us -> 47.9 us
  local copies, waits for them, and re-layouts: 48.5 us -> 55.1 us
    unnamed x2 -> x0, waiting for transfers between devices: 355 us -> none
    all_to_all x1 -> x3, waiting for transfers between devices: 0.01 us -> 75.2 us  [the longest x1 47.9 us: shards(): lax.all_to_all(token_part.astype(jnp.bfloat16).reshape(ep_size, capacity,...]
    all_to_all x1 -> x3, starting transfers between devices: 9.69 us -> 19.3 us  [the longest x1 9.1 us: shards(): lax.all_to_all(token_part.astype(jnp.bfloat16).reshape(ep_size, capacity,...]
    convert_element_type x0 -> x1, local copies, waits for them, and re-layouts: none -> 9.44 us  [shards(): partial = jnp.stack([jnp.einsum('tc,tf->cf', tokens, common_gate_delta, p...]
  transfers between devices with their start and end apart: 5 -> 6, of which waited for: 3 -> 5; matrix products, arithmetic and copies ran while one was open for 10% -> 24% of each run, Pallas kernels for 0% -> 0%
where the time goes in v1:
time: 392 us; the launch traced here: 390 us
  waiting for transfers between devices  140 us (36%)
  blocking collectives  82.6 us (21%)
  local copies, waits for them, and re-layouts  55.1 us (14%)
  matrix products  47.9 us (12%)
  starting transfers between devices  42.6 us (11%)
  other arithmetic  20.6 us (5%)
    all_to_all x1, blocking collectives, shards(): lax.all_to_all(send_tokens, 'ep', split_axis=0, concat_axis=0, tiled=True)  82.6 us
    all_to_all x1, waiting for transfers between devices, shards(): lax.all_to_all(send_cot, 'ep', split_axis=0, concat_axis=0, tiled=True)  64.1 us
    all_to_all x1, waiting for transfers between devices, shards(): lax.all_to_all(token_part.astype(jnp.bfloat16).reshape(ep_size, capacity,...  47.9 us
    all_to_all x1, waiting for transfers between devices, shards(): lax.all_to_all(partial, 'tp', split_axis=0, concat_axis=0, tiled=True)  23.7 us
    gather x2, local copies, waits for them, and re-layouts, shards(): jnp.take(back_rows.reshape(slots_all, model_width), position, axis=0)  11.6 us
    all_to_all x1, starting transfers between devices, shards(): lax.all_to_all(row_weight.reshape(ep_size, capacity), 'ep', split_axis=0,...  11.6 us
    convert_element_type x1, local copies, waits for them, and re-layouts, shards(): partial = jnp.stack([jnp.einsum('tc,tf->cf', tokens, common_gate_delta, p...  9.44 us
    all_to_all x1, starting transfers between devices, shards(): lax.all_to_all(token_part.astype(jnp.bfloat16).reshape(ep_size, capacity,...  9.1 us
  transfers between devices with their start and end apart: 6, of which 5 were waited for; matrix products, arithmetic and copies ran while one was open for 24% of the time, Pallas kernels for 0%

profile of v1, /device:TPU:6, one launch (start us, length us, event | category | flops | bytes accessed | tf_op | source)
XLA Modules:
  0.0 390.0 jit_solution(9786338503939726734)
XLA Ops:
  0.6 0.0 copy-start
  0.7 0.9 copy.34
  1.6 0.1 eq.26
  1.7 0.1 reshape.155
  1.9 1.2 reduce-window.6
  3.0 0.2 slice_reduce_fusion
  3.3 0.1 fusion.23
  3.4 0.1 mul.93
  3.5 2.4 scatter_custom_fusion
  6.0 0.8 copy.38
  6.8 0.1 reshape.157
  6.9 3.2 gather_fusion
  10.1 0.7 select_n.65
  10.8 11.6 %all-to-all-start = ((f32[32,1,24]{2,1,0:T(1,128)}), f32[32,1,24]{2,1,0:T(1,128)S(1)}, u32[]{:S(2)}, u32[]{:S(2)}) async-start(f32[32,1,24]{2,1,0:T(1,128)} %bitcast.3), calls=%async_computation | async-start | bytes 32768 | tf_op jit(solution)/shard_map/all_to_all | solution.py:66
  22.4 1.8 fusion.31
  24.2 1.7 fusion.32
  26.0 0.5 fusion.8
  26.5 0.5 multiply_convert_fusion.10
  27.0 0.5 fusion.6
  27.4 0.4 fusion.7
  27.9 2.0 pad_maximum_fusion
  29.9 7.2 %copy.41 = bf16[2048,3,256]{2,1,0:T(4,128)(2,1)} copy(bf16[2048,3,256]{0,2,1:T(8,128)(2,1)} %pad_maximum_fusion) | data formatting | bytes 6291456 | tf_op jit(solution)/shard_map/stack | solution.py:124
  37.1 9.4 %convert_element_type.74 = bf16[32,8,8,768]{3,2,1,0:T(8,128)(2,1)} reshape(bf16[2048,3,256]{2,1,0:T(4,128)(2,1)} %copy.41) | data formatting | bytes 6291456 | tf_op jit(solution)/shard_map/convert_element_type | solution.py:131
  46.5 3.8 copy.42
  50.3 4.5 %all-to-all-start.5 = ((bf16[8,32,8,768]{3,2,1,0:T(8,128)(2,1)}), bf16[8,32,8,768]{3,2,1,0:T(8,128)(2,1)}, u32[]{:S(2)}, u32[]{:S(2)}) async-start(bf16[8,32,8,768]{3,2,1,0:T(8,128)(2,1)} %copy.42), calls=%async_computation.5 | async-start | bytes 6291456 | tf_op jit(solution)/shard_map/all_to_all | solution.py:134
  54.8 1.1 concatenate.10
  56.0 4.3 %gather_fusion.4 = bf16[768,2048]{1,0:T(8,128)(2,1)} fusion(bf16[129,2048]{1,0:T(8,128)(2,1)S(1)} %concatenate.11, s32[1024]{0:T(1024)S(1)} %pad_clamp_fusion.1), kind=kCustom, calls=%fused_computation.1.clone | custom fusion | bytes 6294528 | tf_op jit(solution)/shard_map/jit(_take)/gather | solution.py:57
  60.3 4.4 %gather_fusion.3 = bf16[768,2048]{1,0:T(8,128)(2,1)} fusion(bf16[129,2048]{1,0:T(8,128)(2,1)S(1)} %concatenate.10, s32[1024]{0:T(1024)S(1)} %pad_clamp_fusion.1), kind=kCustom, calls=%fused_computation.clone | custom fusion | bytes 6294528 | tf_op jit(solution)/shard_map/jit(_take)/gather | solution.py:60
  64.6 5.0 %broadcast_select_fusion.1 = (bf16[768,2048]{1,0:T(8,128)(2,1)}, bf16[768,2048]{1,0:T(8,128)(2,1)}) fusion(bf16[768,2048]{1,0:T(8,128)(2,1)} %gather_fusion.3, pred[768]{0:T(1024)(128)(4,1)S(1)} %get-tuple-element.29, bf16[768,2048]{1,0:T(8,128)(2,1)} %gather_fusion.4), kind=kLoop, calls=%fused_computation.14 | loop fusion | flops 3145728 | bytes 12583680 | tf_op jit(solution)/shard_map/jit(_take)/select_n | solution.py:60
  69.6 23.7 %all-to-all-done.5 = bf16[8,32,8,768]{3,2,1,0:T(8,128)(2,1)} async-done(((bf16[8,32,8,768]{3,2,1,0:T(8,128)(2,1)}), bf16[8,32,8,768]{3,2,1,0:T(8,128)(2,1)}, u32[]{:S(2)}, u32[]{:S(2)}) %all-to-all-start.5) | async-done | bytes 3145760 | tf_op jit(solution)/shard_map/all_to_all | solution.py:134
  93.3 82.6 %all_to_all.40 = bf16[32,24,2048]{2,1,0:T(8,128)(2,1)} all-to-all(bf16[32,24,2048]{2,1,0:T(8,128)(2,1)} %bitcast.87), channel_id=1, replica_groups=mesh['ep'=32,'tp'=8] {'ep'}, dimensions={0} | all-to-all | bytes 6291456 | tf_op jit(solution)/shard_map/all_to_all | solution.py:70
  175.9 5.6 %all-to-all-start.1 = ((bf16[32,24,2048]{2,1,0:T(8,128)(2,1)}), bf16[32,24,2048]{2,1,0:T(8,128)(2,1)}, u32[]{:S(2)}, u32[]{:S(2)}) async-start(bf16[32,24,2048]{2,1,0:T(8,128)(2,1)} %bitcast.86), calls=%async_computation.1 | async-start | bytes 6291456 | tf_op jit(solution)/shard_map/all_to_all | solution.py:71
  181.5 0.5 broadcast.165
  182.0 0.7 reduce.8
  182.7 0.1 mul.94
  182.8 3.4 convert_reduce_fusion
  186.2 3.0 fusion.13
  189.2 64.1 %all-to-all-done.1 = bf16[32,24,2048]{2,1,0:T(8,128)(2,1)} async-done(((bf16[32,24,2048]{2,1,0:T(8,128)(2,1)}), bf16[32,24,2048]{2,1,0:T(8,128)(2,1)}, u32[]{:S(2)}, u32[]{:S(2)}) %all-to-all-start.1) | async-done | bytes 3145760 | tf_op jit(solution)/shard_map/all_to_all | solution.py:71
  253.3 5.7 %all-to-all-start.6 = ((f32[32,8,768]{2,1,0:T(8,128)}), f32[32,8,768]{2,1,0:T(8,128)S(1)}, u32[]{:S(2)}, u32[]{:S(2)}) async-start(f32[32,8,768]{2,1,0:T(8,128)} %convert_reduce_fusion), calls=%async_computation.6 | async-start | bytes 1572864 | tf_op jit(solution)/shard_map/all_to_all | solution.py:136
  259.1 4.5 %fusion.16 = f32[768,512]{0,1:T(8,128)S(1)} fusion(bf16[768,2048]{1,0:T(8,128)(2,1)} %bitcast.88, bf16[1,512,2048]{2,1,0:T(8,128)(2,1)} %param.17), kind=kOutput, calls=%fused_computation.35 | convolution fusion | flops 1610612736 | bytes 6815744 | tf_op jit(solution)/shard_map/rd,fd->rf/dot_general | solution.py:18
  263.6 5.9 %multiply_reduce_fusion = (f32[768]{0:T(1024)S(1)}, bf16[768,512]{0,1:T(8,128)(2,1)}, bf16[768,512]{0,1:T(8,128)(2,1)}, bf16[768,512]{0,1:T(8,128)(2,1)}) fusion(f32[768,512]{0,1:T(8,128)S(1)} %fusion.16, f32[768,512]{0,1:T(8,128)S(1)} %copy-done.10, f32[768]{0:T(1024)S(1)} %mul.94, bf16[768,2048]{1,0:T(8,128)(2,1)} %bitcast.5, ...), kind=kOutput, calls=%fused_computation.39 | convolution fusion | flops 1618083072 | bytes 10754048 | tf_op jit(solution)/shard_map/rd,fd->rf/dot_general | solution.py:77
  269.6 0.7 all_to_all.29
  270.2 5.6 %fusion.11 = f32[768,2048]{1,0:T(8,128)} fusion(bf16[768,512]{0,1:T(8,128)(2,1)} %get-tuple-element.31, bf16[1,512,2048]{2,1,0:T(8,128)(2,1)S(1)} %copy-done), kind=kOutput, calls=%fused_computation.30 | convolution fusion | flops 1610612736 | bytes 9175040 | tf_op jit(solution)/shard_map/rf,fd->rd/dot_general | solution.py:81
  275.9 3.7 all-to-all-done.6
  279.5 6.1 %all-to-all-start.4 = ((f32[32,1,24]{2,1,0:T(1,128)}), f32[32,1,24]{2,1,0:T(1,128)S(1)}, u32[]{:S(2)}, u32[]{:S(2)}) async-start(f32[32,1,24]{2,1,0:T(1,128)} %bitcast.13), calls=%async_computation.4 | async-start | bytes 32768 | tf_op jit(solution)/shard_map/all_to_all | solution.py:101
  285.7 7.2 %add_convert_fusion = bf16[768,2048]{1,0:T(8,128)(2,1)} fusion(f32[768,2048]{1,0:T(8,128)} %fusion.11, bf16[768,512]{0,1:T(8,128)(2,1)} %get-tuple-element.32, bf16[1,512,2048]{2,1,0:T(8,128)(2,1)} %param.17), kind=kOutput, calls=%fused_computation.8 | convolution fusion | flops 1613758464 | bytes 12320768 | tf_op jit(solution)/shard_map/rf,fd->rd/dot_general | solution.py:83
  292.8 0.7 all-to-all-done.4
  293.6 9.1 %all-to-all-start.3 = ((bf16[32,24,2048]{2,1,0:T(8,128)(2,1)}), bf16[32,24,2048]{2,1,0:T(8,128)(2,1)}, u32[]{:S(2)}, u32[]{:S(2)}) async-start(bf16[32,24,2048]{2,1,0:T(8,128)(2,1)} %bitcast.92), calls=%async_computation.3 | async-start | bytes 6291456 | tf_op jit(solution)/shard_map/all_to_all | solution.py:94
  302.7 0.1 sub.21
  302.8 1.5 fusion.33
  304.3 1.8 reduce_sum.49
  306.1 5.4 %fusion.3 = bf16[1,512,2048]{2,1,0:T(8,128)(2,1)} fusion(bf16[768,512]{0,1:T(8,128)(2,1)} %get-tuple-element.31, bf16[768,2048]{1,0:T(8,128)(2,1)} %bitcast.89), kind=kOutput, calls=%fused_computation.18 | convolution fusion | flops 1611661312 | bytes 6029312 | tf_op jit(solution)/shard_map/rf,rd->fd/dot_general | solution.py:84
  311.6 3.1 fusion.4
  314.7 5.1 %fusion.5 = bf16[1,512,2048]{2,1,0:T(8,128)(2,1)} fusion(bf16[768,512]{0,1:T(8,128)(2,1)S(1)} %copy-done.11, bf16[768,2048]{1,0:T(8,128)(2,1)} %bitcast.5, f32[768]{0:T(1024)S(1)} %mul.94), kind=kOutput, calls=%fused_computation.20 | convolution fusion | flops 1616379904 | bytes 6032384 | tf_op jit(solution)/shard_map/rf,rd->fd/dot_general | solution.py:90
  319.8 0.7 reduce.9
  320.5 0.1 reshape.164
  320.6 2.3 gather_fusion.2
  322.9 0.1 gather.23
  323.0 0.7 copy.43
  323.7 47.9 %all-to-all-done.3 = bf16[32,24,2048]{2,1,0:T(8,128)(2,1)} async-done(((bf16[32,24,2048]{2,1,0:T(8,128)(2,1)}), bf16[32,24,2048]{2,1,0:T(8,128)(2,1)}, u32[]{:S(2)}, u32[]{:S(2)}) %all-to-all-start.3) | async-done | bytes 3145760 | tf_op jit(solution)/shard_map/all_to_all | solution.py:94
  371.6 7.5 %gather_fusion.1 = bf16[512,2048]{1,0:T(8,128)(2,1)} fusion(bf16[768,2048]{1,0:T(8,128)(2,1)} %bitcast.12, s32[1024]{0:T(1024)S(1)} %pad_clamp_fusion), kind=kCustom, calls=%fused_computation.3 | custom fusion | bytes 4196352 | tf_op jit(solution)/shard_map/jit(_take)/gather | solution.py:106
  379.1 4.1 %gather.21 = bf16[128,4,2048]{2,1,0:T(4,128)(2,1)} reshape(bf16[512,2048]{1,0:T(8,128)(2,1)} %gather_fusion.1) | data formatting | bytes 4194304 | tf_op jit(solution)/shard_map/jit(_take)/gather | solution.py:106
  383.2 5.6 %convert_reduce_fusion.1 = f32[128,2048]{1,0:T(8,128)S(1)} fusion(bf16[128,4,2048]{2,1,0:T(4,128)(2,1)} %gather.21, pred[128,4]{1,0:T(8,128)(4,1)S(1)} %get-tuple-element.26), kind=kLoop, calls=%fused_computation.9 | loop fusion | flops 2883584 | bytes 3146240 | tf_op jit(solution)/shard_map/reduce_sum | solution.py:105
  388.8 1.1 fusion.10
  (40 shorter events, 0.3 us)
Async XLA Ops:
  0.6 185.6 %copy-start = (bf16[1,512,2048]{2,1,0:T(8,128)(2,1)S(1)}, bf16[1,512,2048]{2,1,0:T(8,128)(2,1)}, u32[]{:S(2)}) copy-start(bf16[1,512,2048]{2,1,0:T(8,128)(2,1)} %param.16) | copy-start | bytes 6291460
  0.6 21.8 %copy-start.1 = (bf16[128,2048]{1,0:T(8,128)(2,1)S(1)}, bf16[128,2048]{1,0:T(8,128)(2,1)}, u32[]{:S(2)}) copy-start(bf16[128,2048]{1,0:T(8,128)(2,1)} %param.12) | copy-start | bytes 1572868
  6.9 19.0 %copy-start.6 = (bf16[128,2048]{1,0:T(8,128)(2,1)S(1)}, bf16[128,2048]{1,0:T(8,128)(2,1)}, u32[]{:S(2)}) copy-start(bf16[128,2048]{1,0:T(8,128)(2,1)} %param.15) | copy-start | bytes 1572868
  10.8 39.5 %all-to-all-start = ((f32[32,1,24]{2,1,0:T(1,128)}), f32[32,1,24]{2,1,0:T(1,128)S(1)}, u32[]{:S(2)}, u32[]{:S(2)}) async-start(f32[32,1,24]{2,1,0:T(1,128)} %bitcast.3), calls=%async_computation | async-start | bytes 32768 | tf_op jit(solution)/shard_map/all_to_all | solution.py:66
  22.4 4.0 %copy-start.8 = (bf16[256,2048]{1,0:T(8,128)(2,1)S(1)}, bf16[256,2048]{1,0:T(8,128)(2,1)}, u32[]{:S(2)}) copy-start(bf16[256,2048]{1,0:T(8,128)(2,1)} %param.21) | copy-start | bytes 3145732
  50.3 43.0 %all-to-all-start.5 = ((bf16[8,32,8,768]{3,2,1,0:T(8,128)(2,1)}), bf16[8,32,8,768]{3,2,1,0:T(8,128)(2,1)}, u32[]{:S(2)}, u32[]{:S(2)}) async-start(bf16[8,32,8,768]{3,2,1,0:T(8,128)(2,1)} %copy.42), calls=%async_computation.5 | async-start | bytes 6291456 | tf_op jit(solution)/shard_map/all_to_all | solution.py:134
  175.9 77.4 %all-to-all-start.1 = ((bf16[32,24,2048]{2,1,0:T(8,128)(2,1)}), bf16[32,24,2048]{2,1,0:T(8,128)(2,1)}, u32[]{:S(2)}, u32[]{:S(2)}) async-start(bf16[32,24,2048]{2,1,0:T(8,128)(2,1)} %bitcast.86), calls=%async_computation.1 | async-start | bytes 6291456 | tf_op jit(solution)/shard_map/all_to_all | solution.py:71
  182.8 3.4 copy-start.3
  253.3 26.2 %all-to-all-start.6 = ((f32[32,8,768]{2,1,0:T(8,128)}), f32[32,8,768]{2,1,0:T(8,128)S(1)}, u32[]{:S(2)}, u32[]{:S(2)}) async-start(f32[32,8,768]{2,1,0:T(8,128)} %convert_reduce_fusion), calls=%async_computation.6 | async-start | bytes 1572864 | tf_op jit(solution)/shard_map/all_to_all | solution.py:136
  259.1 4.6 %copy-start.7 = (bf16[1,512,2048]{2,1,0:T(8,128)(2,1)S(1)}, bf16[1,512,2048]{2,1,0:T(8,128)(2,1)}, u32[]{:S(2)}) copy-start(bf16[1,512,2048]{2,1,0:T(8,128)(2,1)} %param.18) | copy-start | bytes 6291460
  259.1 4.6 %copy-start.10 = (f32[768,512]{0,1:T(8,128)S(1)}, f32[768,512]{0,1:T(8,128)}, u32[]{:S(2)}) copy-start(f32[768,512]{0,1:T(8,128)} %fusion.13) | copy-start | bytes 4718596
  279.5 13.3 %copy-start.5 = (f32[32,8,768]{2,1,0:T(8,128)}, f32[32,8,768]{2,1,0:T(8,128)S(1)}, u32[]{:S(2)}) copy-start(f32[32,8,768]{2,1,0:T(8,128)S(1)} %all-to-all-done.6) | copy-start | bytes 2359300
  279.5 14.0 %all-to-all-start.4 = ((f32[32,1,24]{2,1,0:T(1,128)}), f32[32,1,24]{2,1,0:T(1,128)S(1)}, u32[]{:S(2)}, u32[]{:S(2)}) async-start(f32[32,1,24]{2,1,0:T(1,128)} %bitcast.13), calls=%async_computation.4 | async-start | bytes 32768 | tf_op jit(solution)/shard_map/all_to_all | solution.py:101
  293.6 78.0 %all-to-all-start.3 = ((bf16[32,24,2048]{2,1,0:T(8,128)(2,1)}), bf16[32,24,2048]{2,1,0:T(8,128)(2,1)}, u32[]{:S(2)}, u32[]{:S(2)}) async-start(bf16[32,24,2048]{2,1,0:T(8,128)(2,1)} %bitcast.92), calls=%async_computation.3 | async-start | bytes 6291456 | tf_op jit(solution)/shard_map/all_to_all | solution.py:94
  306.1 5.4 %copy-start.4 = (bf16[32,24,2048]{2,1,0:T(8,128)(2,1)S(1)}, bf16[32,24,2048]{2,1,0:T(8,128)(2,1)}, u32[]{:S(2)}) copy-start(bf16[32,24,2048]{2,1,0:T(8,128)(2,1)} %all_to_all.40) | copy-start | bytes 9437188
  306.1 5.4 %copy-start.9 = (bf16[768,512]{0,1:T(8,128)(2,1)S(1)}, bf16[768,512]{0,1:T(8,128)(2,1)}, u32[]{:S(2)}) copy-start(bf16[768,512]{0,1:T(8,128)(2,1)} %get-tuple-element.32) | copy-start | bytes 2359300
  311.5 3.1 copy-start.11
  383.2 5.6 %copy-start.2 = (bf16[256,2048]{1,0:T(8,128)(2,1)S(1)}, bf16[256,2048]{1,0:T(8,128)(2,1)}, u32[]{:S(2)}) copy-start(bf16[256,2048]{1,0:T(8,128)(2,1)} %param.20) | copy-start | bytes 3145732
